TPU v7x, 256 devices: a whole 4x4x8 slice. The times are simulated.
256 devices in a mesh: fs: 32 (over z, x), tp: 8 (over y, core).
Axes of the slice: x: 4, y: 4, z: 8, core: 2. Of those that a mesh axis runs over, the one named last changes fastest.
Arguments:
- tokens: bfloat16 [32768, 2048], P('fs', 'tp'), may hold values from -6 to 6
- grad_out: bfloat16 [32768, 2048], P('fs', 'tp'), may hold values from -6 to 6
- norm_gain: float32 [2048], replicated, may hold values from 0.1 to 1.9
- gate_weight: bfloat16 [3072, 2048], P('tp', 'fs'), may hold values from -0.125 to 0.125
- up_weight: bfloat16 [3072, 2048], P('tp', 'fs'), may hold values from -0.125 to 0.125
- down_weight: bfloat16 [3072, 2048], P('tp', 'fs'), may hold values from -0.109375 to 0.109375
Outputs:
- grad_input: bfloat16 [32768, 2048], P('fs', 'tp')
- grad_gate: float32 [3072, 2048], P('tp', 'fs')
- grad_up: float32 [3072, 2048], P('tp', 'fs')
- grad_down: float32 [3072, 2048], P('tp', 'fs')
- row_squares: float32 [3, 3072], P(None, 'tp')
All inputs are finite; a program needn't handle non-finite values.
Results may differ from a plain program's by a relative error of at most 0.015.
Values may be sent and summed in bfloat16 or wider, within the bound.
A program may use at most 64 MiB of HBM per device.

v0:
```python
import jax
import jax.numpy as jnp
from jax import lax
from jax.sharding import Mesh
from jax.sharding import PartitionSpec as P

FS = ("fs_0", "fs_1")


def sent_together(arrays, axis, dim, along):
    widths = [a.shape[along] for a in arrays]
    both = jnp.concatenate(arrays, axis=along)
    whole = lax.all_gather(both, axis, axis=dim, tiled=True)
    return tuple(jnp.split(whole, [sum(widths[:k]) for k in range(1, len(widths))], axis=along))


def gather_turned(arrays, axis, dims):
    turned = [jnp.moveaxis(a, dim, 0) for a, dim in zip(arrays, dims)]
    widths = [t[0].size for t in turned]
    both = jnp.concatenate([t.reshape(-1, w) for t, w in zip(turned, widths)], axis=1)
    whole = lax.all_gather(both, axis, axis=0, tiled=True)
    parts = jnp.split(whole, [sum(widths[:k]) for k in range(1, len(widths))], axis=1)
    return tuple(
        (
            jnp.moveaxis(b.reshape(-1, *t.shape[1:]), 0, dim)
            for b, t, dim in zip(parts, turned, dims)
        )
    )


def summed_rows(x, axes, dim):
    if not axes:
        return x
    nearer = lax.psum_scatter(x, axes[0], scatter_dimension=dim, tiled=True)
    return summed_rows(nearer, axes[1:], dim)


def in_blocks(x, dim, peers):
    before, after = (x.shape[:dim], x.shape[dim + 1 :])
    return jnp.moveaxis(x.reshape(*before, peers, -1, *after), dim, 0)


def sum_at_owner(x, axis, dim):
    peers = lax.axis_size(axis)
    parts = lax.all_to_all(in_blocks(x, dim, peers), axis, 0, 0, tiled=True)
    return jnp.sum(parts.astype(jnp.float32), axis=0)


def copy_for_each(x, axis):
    peers = lax.axis_size(axis)
    return lax.all_to_all(jnp.broadcast_to(x[None], (peers, *x.shape)), axis, 0, 0, tiled=True)


def taken_together(x, axis):
    everything = copy_for_each(x, axis)
    return jnp.sum(everything, axis=0)


def in_one(arrays, axis):
    line, at, gathered = (jnp.concatenate([a.reshape(-1) for a in arrays]), 0, [])
    total = taken_together(line, axis)
    for a in arrays:
        gathered.append(total[at : at + a.size].reshape(a.shape))
        at += a.size
    return tuple(gathered)


def contract(left, right, left_dim, right_dim):
    return lax.dot_general(
        left, right, (((left_dim,), (right_dim,)), ((), ())), preferred_element_type=jnp.float32
    )


def rms_back(grad_rows, unit_rows, inv_rms, gain_rows):
    scaled = gain_rows * grad_rows
    inner = jnp.mean(scaled * unit_rows, axis=-1, keepdims=True)
    return inv_rms * (scaled - unit_rows * inner)


def on_device(tokens, grad_out, norm_gain, gate_weight, up_weight, down_weight):
    full_tokens, full_grad = sent_together((tokens, grad_out), "tp", 1, 0)
    floated = full_tokens.astype(jnp.float32)
    inv_rms = lax.rsqrt(jnp.mean(floated * floated, axis=-1, keepdims=True) + 1e-06)
    unit_rows = floated * inv_rms
    gain_rows = norm_gain[None, :]
    normed = (unit_rows * gain_rows).astype(jnp.bfloat16)
    gate_full, up_full, down_full = gather_turned(
        (gate_weight, up_weight, down_weight), FS, (1, 1, 1)
    )
    grad_hidden = 0.5 * contract(full_grad, down_full, 1, 1)
    factor = (full_tokens.shape[0] * lax.axis_size(FS)) ** (-0.5)
    gate_pre = contract(normed, gate_full, 1, 1)
    up_pre = contract(normed, up_full, 1, 1)
    sigma = jax.nn.sigmoid(gate_pre)
    active = gate_pre * sigma
    hidden = (active * up_pre).astype(jnp.bfloat16)
    term_down = 0.5 * factor * contract(hidden, full_grad, 0, 0)
    grad_down = summed_rows(term_down.astype(jnp.bfloat16), FS, 1).astype(jnp.float32)
    gate_grad_pre = (grad_hidden * up_pre * sigma * (1.0 + gate_pre * (1.0 - sigma))).astype(
        jnp.bfloat16
    )
    term_gate = factor * contract(gate_grad_pre, normed, 0, 0)
    grad_gate = summed_rows(term_gate.astype(jnp.bfloat16), FS, 1).astype(jnp.float32)
    up_grad_pre = (grad_hidden * active).astype(jnp.bfloat16)
    term_up = factor * contract(up_grad_pre, normed, 0, 0)
    grad_up = sum_at_owner(term_up.astype(jnp.bfloat16), FS, 1)
    grad_rows = jnp.dot(gate_grad_pre, gate_full, preferred_element_type=jnp.float32)
    grad_rows = grad_rows + jnp.dot(up_grad_pre, up_full, preferred_element_type=jnp.float32)
    partial_value = rms_back(grad_rows, unit_rows, inv_rms, gain_rows)
    summed = sum_at_owner(partial_value.astype(jnp.bfloat16), "tp", 1)
    grad_input = (grad_out.astype(jnp.float32) + summed).astype(jnp.bfloat16)
    width_total = gate_weight.shape[1] * lax.axis_size(FS)
    gate_rows, up_rows, down_rows = in_one(
        (
            jnp.sum(grad_gate * grad_gate, axis=1),
            jnp.sum(grad_up * grad_up, axis=1),
            jnp.sum(grad_down * grad_down, axis=1),
        ),
        FS,
    )
    row_squares = jnp.stack([gate_rows, up_rows, down_rows]) / width_total
    return (grad_input, grad_gate, grad_up, grad_down, row_squares)


def solution(mesh):
    split = Mesh(mesh.devices.reshape(8, 4, mesh.shape["tp"]), ("fs_0", "fs_1", "tp"))
    return jax.shard_map(
        on_device,
        mesh=split,
        in_specs=(P(FS, "tp"), P(FS, "tp"), P(), P("tp", FS), P("tp", FS), P("tp", FS)),
        out_specs=(P(FS, "tp"), P("tp", FS), P("tp", FS), P("tp", FS), P(None, "tp")),
        check_vma=False,
    )
```

profile of v0, /device:TPU:8, one launch (start us, length us, event | category | flops | bytes accessed | tf_op | source)
XLA Modules:
  0.0 353.0 jit_solution(1920257956523172577)
XLA Ops:
  7.2 2.3 pad_maximum_fusion
  11.2 57.5 %all-gather.3.cloned.1.call-done = bf16[2048,2048]{1,0:T(8,128)(2,1)} async-done(((bf16[2048,256]{1,0:T(8,128)(2,1)}), bf16[2048,2048]{1,0:T(8,128)(2,1)}) %all-gather.3.cloned.1.call-update) | async-done | bytes 8388624 | tf_op jit(solution)/shard_map/all_gather | solution.py:13
  68.7 3.1 fusion.8
  71.8 84.1 %all-gather.5.cloned.1.call-done = bf16[2048,1152]{1,0:T(8,128)(2,1)} async-done(((bf16[64,1152]{1,0:T(8,128)(2,1)}), bf16[2048,1152]{1,0:T(8,128)(2,1)}) %all-gather.5.cloned.1.call-update) | async-done | bytes 4718608 | tf_op jit(solution)/shard_map/all_gather | solution.py:21
  155.8 5.2 %fusion.19 = f32[1024,384]{1,0:T(8,128)S(1)} fusion(bf16[2048,1152]{1,0:T(8,128)(2,1)} %all-gather.5.cloned.1.call-done, f32[2048]{0:T(1024)S(1)} %copy-done.2, f32[1024]{0:T(1024)S(1)} %add_rsqrt_fusion, bf16[2048,2048]{1,0:T(8,128)(2,1)} %all-gather.3.cloned.1.call-done), kind=kOutput, calls=%fused_computation.30 | convolution fusion | flops 1619001344 | bytes 7352320 | tf_op jit(solution)/shard_map/dot_general | solution.py:69
  161.1 5.2 %fusion.22 = f32[1024,384]{1,0:T(8,128)S(1)} fusion(bf16[2048,1152]{1,0:T(8,128)(2,1)} %all-gather.5.cloned.1.call-done, f32[2048]{0:T(1024)S(1)} %copy-done.2, f32[1024]{0:T(1024)S(1)} %add_rsqrt_fusion, bf16[2048,2048]{1,0:T(8,128)(2,1)} %all-gather.3.cloned.1.call-done), kind=kOutput, calls=%fused_computation.33 | convolution fusion | flops 1619001344 | bytes 7352320 | tf_op jit(solution)/shard_map/dot_general | solution.py:69
  166.3 3.1 multiply_convert_fusion
  169.4 5.9 %multiply_convert_fusion.4 = (bf16[1024,384]{1,0:T(8,128)(2,1)S(1)}, bf16[1024,384]{1,0:T(8,128)(2,1)S(1)}) fusion(f32[1024,384]{1,0:T(8,128)S(1)} %fusion.19, f32[1024,384]{1,0:T(8,128)} %copy-done.3, bf16[2048,1152]{1,0:T(8,128)(2,1)} %all-gather.5.cloned.1.call-done, bf16[2048,2048]{1,0:T(8,128)(2,1)} %all-gather.3.cloned.1.call-done), kind=kOutput, calls=%fused_computation.24 | convolution fusion | flops 1616117760 | bytes 10485760 | tf_op jit(solution)/shard_map/dot_general | solution.py:69
  175.3 4.2 %multiply_convert_fusion.1 = bf16[384,2048]{1,0:T(8,128)(2,1)S(1)} fusion(bf16[1024,384]{1,0:T(8,128)(2,1)S(1)} %get-tuple-element.30, f32[2048]{0:T(1024)S(1)} %copy-done.2, f32[1024]{0:T(1024)S(1)} %add_rsqrt_fusion, bf16[2048,2048]{1,0:T(8,128)(2,1)} %all-gather.3.cloned.1.call-done), kind=kOutput, calls=%fused_computation.20 | convolution fusion | flops 1620574208 | bytes 6565888 | tf_op jit(solution)/shard_map/dot_general | solution.py:69
  181.1 5.7 %all-to-all-start.1 = ((bf16[32,384,64]{1,2,0:T(8,128)(2,1)}), bf16[32,384,64]{1,2,0:T(8,128)(2,1)S(1)}, u32[]{:S(2)}, u32[]{:S(2)}) async-start(bf16[32,384,64]{1,2,0:T(8,128)(2,1)} %bitcast.5), calls=%async_computation.2 | async-start | bytes 3145728 | tf_op jit(solution)/shard_map/all_to_all | solution.py:45
  187.0 5.4 %multiply_convert_fusion.2 = bf16[384,2048]{1,0:T(8,128)(2,1)} fusion(bf16[1024,384]{1,0:T(8,128)(2,1)S(1)} %get-tuple-element.31, f32[2048]{0:T(1024)S(1)} %copy-done.2, f32[1024]{0:T(1024)S(1)} %add_rsqrt_fusion, bf16[2048,2048]{1,0:T(8,128)(2,1)} %all-gather.3.cloned.1.call-done), kind=kOutput, calls=%fused_computation.21 | convolution fusion | flops 1620574208 | bytes 6565888 | tf_op jit(solution)/shard_map/dot_general | solution.py:69
  192.5 3.9 %fusion.17 = f32[1024,2048]{1,0:T(8,128)S(1)} fusion(bf16[1024,384]{1,0:T(8,128)(2,1)S(1)} %get-tuple-element.31, bf16[2048,1152]{1,0:T(8,128)(2,1)} %all-gather.5.cloned.1.call-done), kind=kOutput, calls=%fused_computation.28 | convolution fusion | flops 1610612736 | bytes 10747904 | tf_op jit(solution)/shard_map/dot_general | solution.py:107
  196.4 5.7 %fusion.4 = (f32[1024]{0:T(1024)S(1)}, f32[1024,2048]{1,0:T(8,128)S(1)}) fusion(f32[1024]{0:T(1024)S(1)} %add_rsqrt_fusion, bf16[2048,2048]{1,0:T(8,128)(2,1)} %all-gather.3.cloned.1.call-done, f32[1024,2048]{1,0:T(8,128)S(1)} %fusion.17, bf16[1024,384]{1,0:T(8,128)(2,1)S(1)} %get-tuple-element.30, bf16[2048,1152]{1,0:T(8,128)(2,1)} %all-gather.5.cloned.1.call-done, ...), kind=kOutput, calls=%fused_computation.6 | convolution fusion | flops 1623194624 | bytes 23347200 | tf_op jit(solution)/shard_map/dot_general | solution.py:108
  202.1 1.8 fusion.7
  203.9 2.2 copy.39
  206.2 25.9 %all-to-all-done.1 = bf16[32,384,64]{1,2,0:T(8,128)(2,1)S(1)} async-done(((bf16[32,384,64]{1,2,0:T(8,128)(2,1)}), bf16[32,384,64]{1,2,0:T(8,128)(2,1)S(1)}, u32[]{:S(2)}, u32[]{:S(2)}) %all-to-all-start.1) | async-done | bytes 1572896 | tf_op jit(solution)/shard_map/all_to_all | solution.py:45
  232.1 5.1 %all-to-all-start = ((bf16[8,1024,256]{2,1,0:T(8,128)(2,1)}), bf16[8,1024,256]{2,1,0:T(8,128)(2,1)}, u32[]{:S(2)}, u32[]{:S(2)}) async-start(bf16[8,1024,256]{2,1,0:T(8,128)(2,1)} %bitcast.25), calls=%async_computation | async-start | bytes 8388608 | tf_op jit(solution)/shard_map/all_to_all | solution.py:45
  237.3 1.7 copy.31
  239.1 34.6 %reduce-scatter.9.cloned.1.call-done = bf16[384,256]{1,0:T(8,128)(2,1)} async-done(((bf16[384,2048]{1,0:T(8,128)(2,1)}), bf16[384,256]{1,0:T(8,128)(2,1)}) %reduce-scatter.9.cloned.1.call-update) | async-done | bytes 196624 | tf_op jit(solution)/shard_map/reduce_scatter | solution.py:34
  275.7 22.2 %reduce-scatter.15.cloned.1.call-done = bf16[64,384]{1,0:T(8,128)(2,1)} async-done(((bf16[256,384]{1,0:T(8,128)(2,1)}), bf16[64,384]{1,0:T(8,128)(2,1)}) %reduce-scatter.15.cloned.1.call-update) | async-done | bytes 49168
  299.6 24.4 %reduce-scatter.13.cloned.1.call-done = bf16[64,384]{1,0:T(8,128)(2,1)} async-done(((bf16[256,384]{1,0:T(8,128)(2,1)}), bf16[64,384]{1,0:T(8,128)(2,1)}) %reduce-scatter.13.cloned.1.call-update) | async-done | bytes 49168
  326.5 8.3 %all-to-all-start.2 = ((f32[32,1,1152]{2,1,0:T(1,128)}), f32[32,1,1152]{2,1,0:T(1,128)S(1)}, u32[]{:S(2)}, u32[]{:S(2)}) async-start(f32[32,1,1152]{2,1,0:T(1,128)} %broadcast_in_dim.2), calls=%async_computation.4 | async-start | bytes 294912 | tf_op jit(solution)/shard_map/all_to_all | solution.py:51
  334.8 2.9 convert_reduce_fusion
  338.6 6.7 %all-to-all-done.2 = f32[32,1,1152]{2,1,0:T(1,128)S(1)} async-done(((f32[32,1,1152]{2,1,0:T(1,128)}), f32[32,1,1152]{2,1,0:T(1,128)S(1)}, u32[]{:S(2)}, u32[]{:S(2)}) %all-to-all-start.2) | async-done | bytes 147488 | tf_op jit(solution)/shard_map/all_to_all | solution.py:51
  (53 shorter events, 11.5 us)
Async XLA Ops:
  7.2 148.7 %copy-start.2 = (f32[2048]{0:T(1024)S(1)}, f32[2048]{0:T(1024)}, u32[]{:S(2)}) copy-start(f32[2048]{0:T(1024)} %param.8) | copy-start | bytes 24580
  7.2 61.5 %all-gather.3.cloned.1.call-start = ((), (), s32[]{:S(2)}) async-start(), calls=%async_computation.7 | async-start | bytes 9437184 | tf_op jit(solution)/shard_map/all_gather | solution.py:13
  9.5 146.3 %all-gather.5.cloned.1.call-start = ((), (), s32[]{:S(2)}) async-start(), calls=%async_computation.8 | async-start | bytes 4866048 | tf_op jit(solution)/shard_map/all_gather | solution.py:21
  11.1 226.1 %reduce-scatter.11.cloned.1.call-start = ((), (), s32[]{:S(2)}) async-start(), calls=%async_computation.10 | async-start | bytes 1769472 | tf_op jit(solution)/shard_map/reduce_scatter | solution.py:34
  155.8 10.4 %slice-start = ((s8[8388608]{0:T(1024)(128)(4,1)}), s8[4194304]{0:T(1024)(128)(4,1)S(1)}, s32[]{:S(2)}) async-start(s8[8388608]{0:T(1024)(128)(4,1)} %bitcast.21), calls=%async_computation.13 | async-start | bytes 8388608
  161.1 5.2 %slice-start.1 = ((s8[8388608]{0:T(1024)(128)(4,1)}), s8[4194304]{0:T(1024)(128)(4,1)S(1)}, s32[]{:S(2)}) async-start(s8[8388608]{0:T(1024)(128)(4,1)} %bitcast.21), calls=%async_computation.14 | async-start | bytes 8388608
  166.3 3.1 copy-start.3
  181.1 51.0 %all-to-all-start.1 = ((bf16[32,384,64]{1,2,0:T(8,128)(2,1)}), bf16[32,384,64]{1,2,0:T(8,128)(2,1)S(1)}, u32[]{:S(2)}, u32[]{:S(2)}) async-start(bf16[32,384,64]{1,2,0:T(8,128)(2,1)} %bitcast.5), calls=%async_computation.2 | async-start | bytes 3145728 | tf_op jit(solution)/shard_map/all_to_all | solution.py:45
  186.8 86.8 %reduce-scatter.9.cloned.1.call-start = ((), (), s32[]{:S(2)}) async-start(), calls=%async_computation.9 | async-start | bytes 1769472 | tf_op jit(solution)/shard_map/reduce_scatter | solution.py:34
  192.4 9.6 %slice-start.2 = ((s8[8388608]{0:T(1024)(128)(4,1)}), s8[4194304]{0:T(1024)(128)(4,1)S(1)}, s32[]{:S(2)}) async-start(s8[8388608]{0:T(1024)(128)(4,1)} %bitcast.23), calls=%async_computation.15 | async-start | bytes 8388608
  196.4 5.7 %slice-start.3 = ((s8[8388608]{0:T(1024)(128)(4,1)}), s8[4194304]{0:T(1024)(128)(4,1)S(1)}, s32[]{:S(2)}) async-start(s8[8388608]{0:T(1024)(128)(4,1)} %bitcast.23), calls=%async_computation.16 | async-start | bytes 8388608
  232.1 93.7 %all-to-all-start = ((bf16[8,1024,256]{2,1,0:T(8,128)(2,1)}), bf16[8,1024,256]{2,1,0:T(8,128)(2,1)}, u32[]{:S(2)}, u32[]{:S(2)}) async-start(bf16[8,1024,256]{2,1,0:T(8,128)(2,1)} %bitcast.25), calls=%async_computation | async-start | bytes 8388608 | tf_op jit(solution)/shard_map/all_to_all | solution.py:45
  237.2 60.7 %reduce-scatter.15.cloned.1.call-start = ((), (), s32[]{:S(2)}) async-start(), calls=%async_computation.12 | async-start | bytes 245760
  239.0 84.9 %reduce-scatter.13.cloned.1.call-start = ((), (), s32[]{:S(2)}) async-start(), calls=%async_computation.11 | async-start | bytes 245760
  275.4 62.3 %copy-start = (bf16[1024,256]{1,0:T(8,128)(2,1)S(1)}, bf16[1024,256]{1,0:T(8,128)(2,1)}, u32[]{:S(2)}) copy-start(bf16[1024,256]{1,0:T(8,128)(2,1)} %param.7) | copy-start | bytes 1572868
  275.6 63.0 %copy-start.1 = (f32[384,64]{0,1:T(8,128)}, f32[384,64]{0,1:T(8,128)S(1)}, u32[]{:S(2)}) copy-start(f32[384,64]{0,1:T(8,128)S(1)} %convert_reduce_fusion.1) | copy-start | bytes 294916
  326.5 18.9 %all-to-all-start.2 = ((f32[32,1,1152]{2,1,0:T(1,128)}), f32[32,1,1152]{2,1,0:T(1,128)S(1)}, u32[]{:S(2)}, u32[]{:S(2)}) async-start(f32[32,1,1152]{2,1,0:T(1,128)} %broadcast_in_dim.2), calls=%async_computation.4 | async-start | bytes 294912 | tf_op jit(solution)/shard_map/all_to_all | solution.py:51
Sparse Core Ops, SparseCore 0:
  9.8 58.8 all-gather.2
  71.8 83.9 all-gather.4
  169.5 56.4 reduce-scatter.10
  228.4 45.1 reduce-scatter.8
  276.0 21.8 reduce-scatter.14
  300.8 23.0 reduce-scatter.12
where the time goes:
time: 354 us; the launch traced here: 353 us
  waiting for transfers between devices  256 us (72%)
  matrix products  38.6 us (11%)
  starting transfers between devices  19.5 us (6%)
  between operations  14.4 us (4%)
  other arithmetic  13.6 us (4%)
  local copies, waits for them, and re-layouts  11.4 us (3%)
    all_gather x1, waiting for transfers between devices, gather_turned(): whole = lax.all_gather(both, axis, axis=0, tiled=True)  84.1 us
    all_gather x1, waiting for transfers between devices, sent_together(): whole = lax.all_gather(both, axis, axis=dim, tiled=True)  57.5 us
    unnamed x8, waiting for transfers between devices  46.7 us
    reduce_scatter x2, waiting for transfers between devices, summed_rows(): nearer = lax.psum_scatter(x, axes[0], scatter_dimension=dim, tiled=True)  34.6 us
    dot_general x6, matrix products, contract(): lax.dot_general(left, right, (((left_dim,), (right_dim,)), ((), ())), pre...  29 us
    all_to_all x2, waiting for transfers between devices, sum_at_owner(): parts = lax.all_to_all(in_blocks(x, dim, peers), axis, 0, 0, tiled=True)  25.9 us
    all_to_all x2, starting transfers between devices, sum_at_owner(): parts = lax.all_to_all(in_blocks(x, dim, peers), axis, 0, 0, tiled=True)  10.8 us
    all_to_all x1, starting transfers between devices, copy_for_each(): lax.all_to_all(jnp.broadcast_to(x[None], (peers, *x.shape)), axis, 0, 0,...  8.32 us
  transfers between devices with their start and end apart: 9, of which 7 were waited for; matrix products, arithmetic and copies ran while one was open for 13% of the time, Pallas kernels for 0%

commit v1 on v0

--- a/solution.py
+++ b/solution.py
@@ -18,7 +18,9 @@
     turned = [jnp.moveaxis(a, dim, 0) for a, dim in zip(arrays, dims)]
     widths = [t[0].size for t in turned]
     both = jnp.concatenate([t.reshape(-1, w) for t, w in zip(turned, widths)], axis=1)
-    whole = lax.all_gather(both, axis, axis=0, tiled=True)
+    whole = jnp.concatenate(
+        lax.all_to_all(jnp.stack([both] * lax.axis_size(axis)), axis, 0, 0), axis=0
+    )
     parts = jnp.split(whole, [sum(widths[:k]) for k in range(1, len(widths))], axis=1)
     return tuple(
         (

time: 354 us -> 324 us (0.915)
  waiting for transfers between devices: 256 us -> 211 us
  starting transfers between devices: 19.5 us -> 33.7 us
    all_gather x1 -> x0, waiting for transfers between devices: 84.1 us -> none  [gather_turned(): whole = lax.all_gather(both, axis, axis=0, tiled=True)]
    all_to_all x0 -> x1, waiting for transfers between devices: none -> 58 us  [gather_turned(): lax.all_to_all(jnp.stack([both] * lax.axis_size(axis)), axis, 0, 0)]
    all_gather x1, waiting for transfers between devices: 57.5 us -> 44 us  [sent_together(): whole = lax.all_gather(both, axis, axis=dim, tiled=True)]
    all_to_all x0 -> x1, starting transfers between devices: none -> 11.4 us  [gather_turned(): lax.all_to_all(jnp.stack([both] * lax.axis_size(axis)), axis, 0, 0)]
    reduce_scatter x2, waiting for transfers between devices: 34.6 us -> 27.3 us  [summed_rows(): nearer = lax.psum_scatter(x, axes[0], scatter_dimension=dim, tiled=True)]
    unnamed x8 -> x7, waiting for transfers between devices: 46.7 us -> 46.6 us
  transfers between devices with their start and end apart: 9 -> 9, of which waited for: 7 -> 7; matrix products, arithmetic and copies ran while one was open for 13% -> 15% of each run, Pallas kernels for 0% -> 0%
where the time goes in v1:
time: 324 us; the launch traced here: 323 us
  waiting for transfers between devices  211 us (65%)
  matrix products  37.1 us (11%)
  starting transfers between devices  33.7 us (10%)
  local copies, waits for them, and re-layouts  14.1 us (4%)
  between operations  14 us (4%)
  other arithmetic  13 us (4%)
    all_to_all x1, waiting for transfers between devices, gather_turned(): lax.all_to_all(jnp.stack([both] * lax.axis_size(axis)), axis, 0, 0)  58 us
    unnamed x7, waiting for transfers between devices  46.6 us
    all_gather x1, waiting for transfers between devices, sent_together(): whole = lax.all_gather(both, axis, axis=dim, tiled=True)  44 us
    all_to_all x2, waiting for transfers between devices, sum_at_owner(): parts = lax.all_to_all(in_blocks(x, dim, peers), axis, 0, 0, tiled=True)  28.3 us
    dot_general x6, matrix products, contract(): lax.dot_general(left, right, (((left_dim,), (right_dim,)), ((), ())), pre...  27.6 us
    reduce_scatter x2, waiting for transfers between devices, summed_rows(): nearer = lax.psum_scatter(x, axes[0], scatter_dimension=dim, tiled=True)  27.3 us
    all_to_all x2, starting transfers between devices, sum_at_owner(): parts = lax.all_to_all(in_blocks(x, dim, peers), axis, 0, 0, tiled=True)  13.8 us
    all_to_all x1, starting transfers between devices, gather_turned(): lax.all_to_all(jnp.stack([both] * lax.axis_size(axis)), axis, 0, 0)  11.4 us
  transfers between devices with their start and end apart: 9, of which 7 were waited for; matrix products, arithmetic and copies ran while one was open for 15% of the time, Pallas kernels for 0%

profile of v1, /device:TPU:8, one launch (start us, length us, event | category | flops | bytes accessed | tf_op | source)
XLA Modules:
  0.0 323.0 jit_solution(10811816415289694159)
XLA Ops:
  7.2 2.3 pad_maximum_fusion
  10.4 2.7 stack.10
  13.1 11.4 %all-to-all-start = ((bf16[32,64,1152]{2,1,0:T(8,128)(2,1)}), bf16[32,64,1152]{2,1,0:T(8,128)(2,1)}, u32[]{:S(2)}, u32[]{:S(2)}) async-start(bf16[32,64,1152]{2,1,0:T(8,128)(2,1)} %stack.10), calls=%async_computation | async-start | bytes 9437184 | tf_op jit(solution)/shard_map/all_to_all | solution.py:22
  24.6 44.0 %all-gather.2.cloned.1.call-done = bf16[2048,2048]{1,0:T(8,128)(2,1)} async-done(((bf16[2048,256]{1,0:T(8,128)(2,1)}), bf16[2048,2048]{1,0:T(8,128)(2,1)}) %all-gather.2.cloned.1.call-update) | async-done | bytes 8388624 | tf_op jit(solution)/shard_map/all_gather | solution.py:13
  68.7 3.1 fusion.8
  71.8 58.0 %all-to-all-done = bf16[32,64,1152]{2,1,0:T(8,128)(2,1)} async-done(((bf16[32,64,1152]{2,1,0:T(8,128)(2,1)}), bf16[32,64,1152]{2,1,0:T(8,128)(2,1)}, u32[]{:S(2)}, u32[]{:S(2)}) %all-to-all-start) | async-done | bytes 4718624 | tf_op jit(solution)/shard_map/all_to_all | solution.py:22
  129.8 5.2 %fusion.19 = f32[1024,384]{1,0:T(8,128)S(1)} fusion(bf16[2048,1152]{1,0:T(8,128)(2,1)} %bitcast.3, f32[2048]{0:T(1024)S(1)} %copy-done.3, f32[1024]{0:T(1024)S(1)} %add_rsqrt_fusion, bf16[2048,2048]{1,0:T(8,128)(2,1)} %all-gather.2.cloned.1.call-done), kind=kOutput, calls=%fused_computation.30 | convolution fusion | flops 1619001344 | bytes 7352320 | tf_op jit(solution)/shard_map/dot_general | solution.py:71
  135.0 3.8 %fusion.22 = f32[1024,384]{1,0:T(8,128)S(1)} fusion(bf16[2048,1152]{1,0:T(8,128)(2,1)} %bitcast.3, f32[2048]{0:T(1024)S(1)} %copy-done.3, f32[1024]{0:T(1024)S(1)} %add_rsqrt_fusion, bf16[2048,2048]{1,0:T(8,128)(2,1)S(1)} %copy-done), kind=kOutput, calls=%fused_computation.33 | convolution fusion | flops 1619001344 | bytes 7352320 | tf_op jit(solution)/shard_map/dot_general | solution.py:71
  138.8 3.1 multiply_convert_fusion
  141.9 5.9 %multiply_convert_fusion.4 = (bf16[1024,384]{1,0:T(8,128)(2,1)S(1)}, bf16[1024,384]{1,0:T(8,128)(2,1)S(1)}) fusion(f32[1024,384]{1,0:T(8,128)S(1)} %fusion.19, f32[1024,384]{1,0:T(8,128)} %copy-done.4, bf16[2048,1152]{1,0:T(8,128)(2,1)} %bitcast.3, bf16[2048,2048]{1,0:T(8,128)(2,1)} %all-gather.2.cloned.1.call-done), kind=kOutput, calls=%fused_computation.24 | convolution fusion | flops 1616117760 | bytes 10485760 | tf_op jit(solution)/shard_map/dot_general | solution.py:71
  147.8 4.2 %multiply_convert_fusion.1 = bf16[384,2048]{1,0:T(8,128)(2,1)S(1)} fusion(bf16[1024,384]{1,0:T(8,128)(2,1)S(1)} %get-tuple-element.30, f32[2048]{0:T(1024)S(1)} %copy-done.3, f32[1024]{0:T(1024)S(1)} %add_rsqrt_fusion, bf16[2048,2048]{1,0:T(8,128)(2,1)} %all-gather.2.cloned.1.call-done), kind=kOutput, calls=%fused_computation.20 | convolution fusion | flops 1620574208 | bytes 6565888 | tf_op jit(solution)/shard_map/dot_general | solution.py:71
  153.6 8.8 %all-to-all-start.2 = ((bf16[32,384,64]{1,2,0:T(8,128)(2,1)}), bf16[32,384,64]{1,2,0:T(8,128)(2,1)S(1)}, u32[]{:S(2)}, u32[]{:S(2)}) async-start(bf16[32,384,64]{1,2,0:T(8,128)(2,1)} %bitcast.6), calls=%async_computation.3 | async-start | bytes 3145728 | tf_op jit(solution)/shard_map/all_to_all | solution.py:47
  162.5 5.4 %multiply_convert_fusion.2 = bf16[384,2048]{1,0:T(8,128)(2,1)} fusion(bf16[1024,384]{1,0:T(8,128)(2,1)S(1)} %get-tuple-element.31, f32[2048]{0:T(1024)S(1)} %copy-done.3, f32[1024]{0:T(1024)S(1)} %add_rsqrt_fusion, bf16[2048,2048]{1,0:T(8,128)(2,1)} %all-gather.2.cloned.1.call-done), kind=kOutput, calls=%fused_computation.21 | convolution fusion | flops 1620574208 | bytes 6565888 | tf_op jit(solution)/shard_map/dot_general | solution.py:71
  167.9 3.9 %fusion.17 = f32[1024,2048]{1,0:T(8,128)S(1)} fusion(bf16[1024,384]{1,0:T(8,128)(2,1)S(1)} %get-tuple-element.31, bf16[2048,1152]{1,0:T(8,128)(2,1)} %bitcast.3), kind=kOutput, calls=%fused_computation.28 | convolution fusion | flops 1610612736 | bytes 10747904 | tf_op jit(solution)/shard_map/dot_general | solution.py:109
  171.9 5.6 %fusion.4 = (f32[1024]{0:T(1024)S(1)}, f32[1024,2048]{1,0:T(8,128)S(1)}) fusion(f32[1024]{0:T(1024)S(1)} %add_rsqrt_fusion, bf16[2048,2048]{1,0:T(8,128)(2,1)} %all-gather.2.cloned.1.call-done, f32[1024,2048]{1,0:T(8,128)S(1)} %fusion.17, bf16[1024,384]{1,0:T(8,128)(2,1)S(1)} %get-tuple-element.30, bf16[2048,1152]{1,0:T(8,128)(2,1)} %bitcast.3, ...), kind=kOutput, calls=%fused_computation.6 | convolution fusion | flops 1623194624 | bytes 23347200 | tf_op jit(solution)/shard_map/dot_general | solution.py:110
  179.4 2.2 copy.39
  181.6 28.3 %all-to-all-done.2 = bf16[32,384,64]{1,2,0:T(8,128)(2,1)S(1)} async-done(((bf16[32,384,64]{1,2,0:T(8,128)(2,1)}), bf16[32,384,64]{1,2,0:T(8,128)(2,1)S(1)}, u32[]{:S(2)}, u32[]{:S(2)}) %all-to-all-start.2) | async-done | bytes 1572896 | tf_op jit(solution)/shard_map/all_to_all | solution.py:47
  210.0 5.0 %all-to-all-start.1 = ((bf16[8,1024,256]{2,1,0:T(8,128)(2,1)}), bf16[8,1024,256]{2,1,0:T(8,128)(2,1)}, u32[]{:S(2)}, u32[]{:S(2)}) async-start(bf16[8,1024,256]{2,1,0:T(8,128)(2,1)} %bitcast.24), calls=%async_computation.1 | async-start | bytes 8388608 | tf_op jit(solution)/shard_map/all_to_all | solution.py:47
  216.8 27.3 %reduce-scatter.9.cloned.1.call-done = bf16[384,256]{1,0:T(8,128)(2,1)} async-done(((bf16[384,2048]{1,0:T(8,128)(2,1)}), bf16[384,256]{1,0:T(8,128)(2,1)}) %reduce-scatter.9.cloned.1.call-update) | async-done | bytes 196624 | tf_op jit(solution)/shard_map/reduce_scatter | solution.py:36
  246.1 22.2 %reduce-scatter.15.cloned.1.call-done = bf16[64,384]{1,0:T(8,128)(2,1)} async-done(((bf16[256,384]{1,0:T(8,128)(2,1)}), bf16[64,384]{1,0:T(8,128)(2,1)}) %reduce-scatter.15.cloned.1.call-update) | async-done | bytes 49168
  270.0 24.3 %reduce-scatter.13.cloned.1.call-done = bf16[64,384]{1,0:T(8,128)(2,1)} async-done(((bf16[256,384]{1,0:T(8,128)(2,1)}), bf16[64,384]{1,0:T(8,128)(2,1)}) %reduce-scatter.13.cloned.1.call-update) | async-done | bytes 49168
  296.9 8.3 %all-to-all-start.3 = ((f32[32,1,1152]{2,1,0:T(1,128)}), f32[32,1,1152]{2,1,0:T(1,128)S(1)}, u32[]{:S(2)}, u32[]{:S(2)}) async-start(f32[32,1,1152]{2,1,0:T(1,128)} %broadcast_in_dim.2), calls=%async_computation.5 | async-start | bytes 294912 | tf_op jit(solution)/shard_map/all_to_all | solution.py:53
  305.2 2.9 convert_reduce_fusion
  309.0 6.8 %all-to-all-done.3 = f32[32,1,1152]{2,1,0:T(1,128)S(1)} async-done(((f32[32,1,1152]{2,1,0:T(1,128)}), f32[32,1,1152]{2,1,0:T(1,128)S(1)}, u32[]{:S(2)}, u32[]{:S(2)}) %all-to-all-start.3) | async-done | bytes 147488 | tf_op jit(solution)/shard_map/all_to_all | solution.py:53
  (50 shorter events, 14.2 us)
Async XLA Ops:
  7.2 61.5 %all-gather.2.cloned.1.call-start = ((), (), s32[]{:S(2)}) async-start(), calls=%async_computation.8 | async-start | bytes 9437184 | tf_op jit(solution)/shard_map/all_gather | solution.py:13
  13.1 116.6 %all-to-all-start = ((bf16[32,64,1152]{2,1,0:T(8,128)(2,1)}), bf16[32,64,1152]{2,1,0:T(8,128)(2,1)}, u32[]{:S(2)}, u32[]{:S(2)}) async-start(bf16[32,64,1152]{2,1,0:T(8,128)(2,1)} %stack.10), calls=%async_computation | async-start | bytes 9437184 | tf_op jit(solution)/shard_map/all_to_all | solution.py:22
  24.6 105.2 %copy-start.3 = (f32[2048]{0:T(1024)S(1)}, f32[2048]{0:T(1024)}, u32[]{:S(2)}) copy-start(f32[2048]{0:T(1024)} %param.8) | copy-start | bytes 24580
  24.6 190.3 %reduce-scatter.11.cloned.1.call-start = ((), (), s32[]{:S(2)}) async-start(), calls=%async_computation.10 | async-start | bytes 1769472 | tf_op jit(solution)/shard_map/reduce_scatter | solution.py:36
  129.8 5.2 %copy-start = (bf16[2048,2048]{1,0:T(8,128)(2,1)S(1)}, bf16[2048,2048]{1,0:T(8,128)(2,1)}, u32[]{:S(2)}) copy-start(bf16[2048,2048]{1,0:T(8,128)(2,1)} %all-gather.2.cloned.1.call-done) | copy-start | bytes 25165828
  138.8 3.1 copy-start.4
  153.6 56.4 %all-to-all-start.2 = ((bf16[32,384,64]{1,2,0:T(8,128)(2,1)}), bf16[32,384,64]{1,2,0:T(8,128)(2,1)S(1)}, u32[]{:S(2)}, u32[]{:S(2)}) async-start(bf16[32,384,64]{1,2,0:T(8,128)(2,1)} %bitcast.6), calls=%async_computation.3 | async-start | bytes 3145728 | tf_op jit(solution)/shard_map/all_to_all | solution.py:47
  162.5 81.6 %reduce-scatter.9.cloned.1.call-start = ((), (), s32[]{:S(2)}) async-start(), calls=%async_computation.9 | async-start | bytes 1769472 | tf_op jit(solution)/shard_map/reduce_scatter | solution.py:36
  167.9 9.6 %slice-start = ((s8[8388608]{0:T(1024)(128)(4,1)}), s8[4194304]{0:T(1024)(128)(4,1)S(1)}, s32[]{:S(2)}) async-start(s8[8388608]{0:T(1024)(128)(4,1)} %bitcast.22), calls=%async_computation.13 | async-start | bytes 8388608
  171.9 5.7 %slice-start.1 = ((s8[8388608]{0:T(1024)(128)(4,1)}), s8[4194304]{0:T(1024)(128)(4,1)S(1)}, s32[]{:S(2)}) async-start(s8[8388608]{0:T(1024)(128)(4,1)} %bitcast.22), calls=%async_computation.14 | async-start | bytes 8388608
  210.0 86.2 %all-to-all-start.1 = ((bf16[8,1024,256]{2,1,0:T(8,128)(2,1)}), bf16[8,1024,256]{2,1,0:T(8,128)(2,1)}, u32[]{:S(2)}, u32[]{:S(2)}) async-start(bf16[8,1024,256]{2,1,0:T(8,128)(2,1)} %bitcast.24), calls=%async_computation.1 | async-start | bytes 8388608 | tf_op jit(solution)/shard_map/all_to_all | solution.py:47
  214.9 53.4 %reduce-scatter.15.cloned.1.call-start = ((), (), s32[]{:S(2)}) async-start(), calls=%async_computation.12 | async-start | bytes 245760
  216.7 77.6 %reduce-scatter.13.cloned.1.call-start = ((), (), s32[]{:S(2)}) async-start(), calls=%async_computation.11 | async-start | bytes 245760
  245.8 62.2 %copy-start.1 = (bf16[1024,256]{1,0:T(8,128)(2,1)S(1)}, bf16[1024,256]{1,0:T(8,128)(2,1)}, u32[]{:S(2)}) copy-start(bf16[1024,256]{1,0:T(8,128)(2,1)} %param.7) | copy-start | bytes 1572868
  246.1 62.9 %copy-start.2 = (f32[384,64]{0,1:T(8,128)}, f32[384,64]{0,1:T(8,128)S(1)}, u32[]{:S(2)}) copy-start(f32[384,64]{0,1:T(8,128)S(1)} %convert_reduce_fusion.1) | copy-start | bytes 294916
  296.9 18.8 %all-to-all-start.3 = ((f32[32,1,1152]{2,1,0:T(1,128)}), f32[32,1,1152]{2,1,0:T(1,128)S(1)}, u32[]{:S(2)}, u32[]{:S(2)}) async-start(f32[32,1,1152]{2,1,0:T(1,128)} %broadcast_in_dim.2), calls=%async_computation.5 | async-start | bytes 294912 | tf_op jit(solution)/shard_map/all_to_all | solution.py:53
Sparse Core Ops, SparseCore 0:
  9.8 58.8 all-gather.1
  142.0 57.7 reduce-scatter.10
  202.4 41.6 reduce-scatter.8
  246.4 21.8 reduce-scatter.14
  271.3 22.9 reduce-scatter.12
